TPU v7x, 32 devices: a whole 2x2x4 slice. The times are simulated.
32 devices in a mesh: dp: 4 (over y, x), kv: 4 (over z), tp: 2 (over core).
Axes of the slice: x: 2, y: 2, z: 4, core: 2. Of those that a mesh axis runs over, the one named last changes fastest.
Arguments:
- tokens: bfloat16 [128, 4096], P('dp', ('kv', 'tp')), parts along dimension 0, may hold values from -12 to 12
- norm_gain: float32 [4096], replicated, may hold values from 0.1 to 1.9
- w_query: bfloat16 [4096, 3072], P(None, ('kv', 'tp')), may hold values from -0.09375 to 0.09375
- w_key: bfloat16 [4096, 3072], P(None, ('kv', 'tp')), may hold values from -0.09375 to 0.09375
- w_value: bfloat16 [4096, 3072], P(None, ('kv', 'tp')), may hold values from -0.09375 to 0.09375
- w_gate: bfloat16 [4096, 3072], P(None, ('kv', 'tp')), may hold values from -0.09375 to 0.09375
- w_output: bfloat16 [3072, 4096], P(None, ('kv', 'tp')), may hold values from -0.109375 to 0.109375
- decay_rate: float32 [24], replicated, may hold values from 0.003 to 2
- state: float32 [32, 24, 128, 128], P(('dp', 'kv', 'tp')), parts along dimension 0, may hold values from -0.54 to 0.54
- prev_keys: bfloat16 [32, 4, 3072], P(('dp', 'kv', 'tp')), parts along dimension 0, may hold values from -0.5390625 to 0.5390625
- prev_values: bfloat16 [32, 4, 3072], P(('dp', 'kv', 'tp')), parts along dimension 0, may hold values from -6 to 6
- accepted: int32 [32], P(('dp', 'kv', 'tp')), parts along dimension 0, may hold values from 0 to 4
- parents: int32 [32, 4], P(('dp', 'kv', 'tp')), parts along dimension 0, may hold values from -1 to 2, as said below
- seq_length: int32 [32], P(('dp', 'kv', 'tp')), parts along dimension 0, may hold values from 1 to 8191
Outputs:
- output: bfloat16 [128, 4096], P('dp', ('kv', 'tp')), parts along dimension 0
- carried: float32 [32, 24, 128, 128], P(('dp', 'kv', 'tp')), parts along dimension 0
There are 4 independent parts, one for each index of `dp`. A program takes and returns all parts, laid end to end along the dimension named above; an argument that names none is the same for every part. Nothing has to cross between parts.
Inputs may be any that keep to these rules, and one draw needn't show every extreme that they name: parents[s, i] is -1 or an earlier proposal of the same sequence; proposal 0 has -1.
All inputs are finite; a program needn't handle non-finite values.
Results may differ from a plain program's by a relative error of at most 0.013.
Values may be sent and summed in bfloat16 or wider, within the bound.
A program may use at most 64 MiB of HBM per device.

v0:
```python
import jax
import jax.numpy as jnp
from jax import lax
from jax.sharding import PartitionSpec as P

EPS = 1e-06
HIGH = lax.Precision.HIGHEST


def rotate(tensor, positions):
    half_dim = tensor.shape[-1] // 2
    frequency = 10000.0 ** (-jnp.arange(half_dim, dtype=jnp.float32) / half_dim)
    angles = positions[:, :, None] * frequency[None, None, :]
    cosine = jnp.cos(angles)[:, :, None, :]
    sine_part = jnp.sin(angles)[:, :, None, :]
    first = tensor[..., :half_dim]
    second = tensor[..., half_dim:]
    return jnp.concatenate(
        [first * cosine - second * sine_part, second * cosine + first * sine_part], axis=-1
    )


def ancestry_of(parents):
    props = parents.shape[1]
    linked = (parents[:, :, None] == jnp.arange(props, dtype=jnp.int32)[None, None, :]).astype(
        jnp.float32
    )
    identity = jnp.broadcast_to(jnp.eye(props, dtype=jnp.float32), linked.shape)
    ancestry = identity
    power = identity
    for hop in range(props - 1):
        power = jnp.einsum("bij,bjk->bik", power, linked, precision=HIGH)
        ancestry = ancestry + power
    depths = jnp.sum(ancestry, axis=-1) - 1.0
    return (ancestry, depths)


def advance(state, prev_keys, prev_values, accepted, decays):
    nseq, props, width = prev_keys.shape
    heads = decays.shape[0]
    head_dim = width // heads
    old_keys = prev_keys.astype(jnp.float32).reshape(nseq, props, heads, head_dim)
    old_values = prev_values.astype(jnp.float32).reshape(nseq, props, heads, head_dim)
    steps_done = accepted.astype(jnp.float32)[:, None]
    index = jnp.arange(props, dtype=jnp.float32)[None, :]
    age = jnp.maximum(steps_done - 1.0 - index, 0.0)
    weights = jnp.where(
        (index < steps_done)[:, :, None], jnp.exp(-decays[None, None, :] * age[:, :, None]), 0.0
    )
    kept = jnp.exp(-decays[None, :] * steps_done)
    added = jnp.einsum("bphd,bphe->bhde", old_keys * weights[..., None], old_values, precision=HIGH)
    return kept[:, :, None, None] * state + added


def retain(queries, key_rows, val_rows, gate_rows, decays, carried, parents, accepted, seq_length):
    nseq, props, heads, head_dim = queries.shape
    ancestry, depths = ancestry_of(parents)
    positions = (seq_length + accepted).astype(jnp.float32)[:, None] + depths
    rotated_q = rotate(queries.astype(jnp.float32), positions)
    rotated_k = rotate(key_rows.astype(jnp.float32), positions) * head_dim ** (-0.5)
    scores = jnp.einsum("bihd,bjhd->bhij", rotated_q, rotated_k, precision=HIGH)
    spacing = jnp.maximum(depths[:, :, None] - depths[:, None, :], 0.0)
    weighting = ancestry[:, None] * jnp.exp(-decays[None, :, None, None] * spacing[:, None])
    within = jnp.einsum(
        "bhij,bjhe->bihe", scores * weighting, val_rows.astype(jnp.float32), precision=HIGH
    )
    state_scale = jnp.exp(-decays[None, None, :] * (depths[:, :, None] + 1.0))
    from_state = (
        jnp.einsum("bihd,bhde->bihe", rotated_q, carried, precision=HIGH) * state_scale[..., None]
    )
    mixed_raw = within + from_state
    average = jnp.mean(mixed_raw, axis=-1, keepdims=True)
    centred = mixed_raw - average
    variance = jnp.mean(centred * centred, axis=-1, keepdims=True)
    normed = (centred * lax.rsqrt(variance + EPS)).reshape(nseq * props, heads * head_dim)
    gates = gate_rows.astype(jnp.float32).reshape(nseq * props, heads * head_dim)
    return (normed * jax.nn.silu(gates)).astype(jnp.bfloat16)


def per_device(
    tokens,
    norm_gain,
    w_query,
    w_key,
    w_value,
    w_gate,
    w_output,
    decay_rate,
    state,
    prev_keys,
    prev_values,
    accepted,
    parents,
    seq_length,
):
    weights = jnp.concatenate([w_query, w_key, w_value, w_gate], axis=1)
    columns = weights.shape[1]
    whole = lax.all_gather(tokens, ("kv", "tp"), axis=1, tiled=True).astype(jnp.float32)
    scale = lax.rsqrt(jnp.mean(whole * whole, axis=1, keepdims=True) + EPS)
    full_normed = (whole * scale * norm_gain[None, :]).astype(jnp.bfloat16)
    projected = jnp.dot(full_normed, weights, preferred_element_type=jnp.float32)
    rows_count = tokens.shape[0]
    projected = projected.astype(jnp.bfloat16).reshape(rows_count, 4, columns // 4)
    regrouped = lax.all_to_all(projected, ("kv", "tp"), split_axis=0, concat_axis=2, tiled=True)
    nseq = state.shape[0]
    heads = decay_rate.shape[0]
    head_dim = state.shape[2]
    props = parents.shape[1]

    def shaped(role):
        return regrouped[:, role].reshape(nseq, props, heads, head_dim)

    carried = advance(state, prev_keys, prev_values, accepted, decay_rate)
    mixed = retain(
        shaped(0),
        shaped(1),
        shaped(2),
        shaped(3),
        decay_rate,
        carried,
        parents,
        accepted,
        seq_length,
    )
    output = jnp.dot(
        lax.all_gather(mixed, ("kv", "tp"), axis=0, tiled=True),
        w_output,
        preferred_element_type=jnp.float32,
    ).astype(jnp.bfloat16)
    return (output, carried)


def solution(mesh):
    placed = (
        P("dp", ("kv", "tp")),
        P(),
        P(None, ("kv", "tp")),
        P(None, ("kv", "tp")),
        P(None, ("kv", "tp")),
        P(None, ("kv", "tp")),
        P(None, ("kv", "tp")),
        P(),
        P(("dp", "kv", "tp"), None, None, None),
        P(("dp", "kv", "tp"), None, None),
        P(("dp", "kv", "tp"), None, None),
        P(("dp", "kv", "tp")),
        P(("dp", "kv", "tp"), None),
        P(("dp", "kv", "tp")),
    )
    return jax.shard_map(
        per_device,
        mesh=mesh,
        in_specs=placed,
        out_specs=(P("dp", ("kv", "tp")), P(("dp", "kv", "tp"), None, None, None)),
        check_vma=False,
    )
```

profile of v0, /device:TPU:0, one launch (start us, length us, event | category | flops | bytes accessed | tf_op | source)
XLA Modules:
  0.0 55.8 jit_solution(4770530740804355256)
XLA Ops:
  0.6 0.0 copy-start
  0.6 16.3 %all_gather.6 = bf16[32,4096]{1,0:T(8,128)(2,1)S(1)} all-gather(bf16[32,512]{1,0:T(8,128)(2,1)} %param.14), channel_id=1, replica_groups=mesh['dp'=4,'kv'=4,'tp'=2] {'kv','tp'}, dimensions={1}, use_global_device_ids=true | all-gather | bytes 294912 | tf_op jit(solution)/shard_map/all_gather | solution.py:98
  16.9 0.2 fusion.20
  17.1 0.0 copy-start.3
  17.1 0.0 copy-start.4
  17.1 0.0 copy-start.1
  17.1 0.0 copy-start.2
  17.1 6.3 %fusion.8 = bf16[32,1536]{1,0:T(8,128)(2,1)S(1)} fusion(bf16[4096,384]{1,0:T(8,128)(2,1)} %param.19, bf16[4096,384]{1,0:T(8,128)(2,1)} %param.18, bf16[4096,384]{1,0:T(8,128)(2,1)} %param.17, bf16[4096,384]{1,0:T(8,128)(2,1)} %param.16, bf16[32,4096]{1,0:T(8,128)(2,1)S(1)} %all_gather.6, f32[4096]{0:T(1024)} %param.15, f32[32]{0:T(128)S(1)} %add_rsqrt_fusion.1), kind=kOutput, calls=%fused_computation.8 | convolution fusion | flops 453558272 | bytes 12959872 | tf_op jit(solution)/shard_map/dot_general | solution.py:101
  23.5 0.7 %reshape.477 = bf16[32,4,384]{2,1,0:T(4,128)(2,1)} reshape(bf16[32,1536]{1,0:T(8,128)(2,1)S(1)} %fusion.8) | data formatting | bytes 196608 | tf_op jit(solution)/shard_map/reshape | solution.py:103
  24.1 4.7 %all-to-all-start = ((bf16[32,4,384]{2,1,0:T(4,128)(2,1)}), bf16[32,4,384]{2,1,0:T(4,128)(2,1)S(1)}, u32[]{:S(2)}, u32[]{:S(2)}) async-start(bf16[32,4,384]{2,1,0:T(4,128)(2,1)} %reshape.477), calls=%async_computation | async-start | bytes 196608 | tf_op jit(solution)/shard_map/all_to_all | solution.py:104
  30.2 0.0 copy-done.3
  30.2 0.0 copy-done.4
  30.2 0.3 fusion.39
  30.4 0.3 fusion.38
  30.7 0.3 fusion.50
  31.0 0.1 copy.41
  31.1 0.1 multiply_cosine_fusion
  31.2 0.1 multiply_exponential_fusion
  31.3 0.0 copy-done.1
  31.3 0.0 copy-done.2
  31.3 4.2 %bitcast_add_fusion = f32[1,24,128,128]{3,2,1,0:T(8,128)} fusion(f32[1,24,128,128]{3,2,1,0:T(8,128)} %param.22, f32[24]{0:T(128)S(1)} %get-tuple-element.23, bf16[1,4,3072]{2,1,0:T(4,128)(2,1)S(1)} %copy-done.1, bf16[1,4,3072]{2,1,0:T(4,128)(2,1)S(1)} %copy-done.2, f32[4,24]{0,1:T(8,128)S(1)} %get-tuple-element.21), kind=kOutput, calls=%fused_computation.11 | convolution fusion | flops 19685376 | bytes 3195360 | tf_op jit(solution)/shard_map/bphd,bphe->bhde/dot_general | solution.py:51
  35.5 0.1 subtract_maximum_fusion
  35.5 0.0 all-to-all-done
  35.6 0.2 slice_reduce_fusion
  35.8 0.1 fusion.47
  35.9 0.1 subtract_bitcast_fusion
  36.0 2.9 %fusion.17 = f32[1,4,24,128]{3,1,2,0:T(4,128)S(1)} fusion(f32[1,24,128,128]{3,2,1,0:T(8,128)} %bitcast_add_fusion, f32[4,24]{0,1:T(8,128)S(1)} %get-tuple-element.20, f32[1,4,24,64]{3,1,2,0:T(4,128)S(1)} %get-tuple-element.14, f32[1,4,24,64]{3,1,2,0:T(4,128)S(1)} %get-tuple-element.15), kind=kOutput, calls=%fused_computation.17 | convolution fusion | flops 18898944 | bytes 1671552 | tf_op jit(solution)/shard_map/bihd,bhde->bihe/dot_general | solution.py:69
  38.8 0.4 convolution_multiply_fusion
  39.2 0.3 fusion.51
  39.5 0.2 multiply_reduce_fusion
  39.7 0.1 fusion.37
  39.8 14.6 %all-gather = bf16[8,4,3072]{2,1,0:T(4,128)(2,1)S(1)} all-gather(bf16[1,4,3072]{2,1,0:T(4,128)(2,1)S(1)} %fusion.37), channel_id=1, replica_groups=mesh['dp'=4,'kv'=4,'tp'=2] {'kv','tp'}, dimensions={0}, use_global_device_ids=true | all-gather | bytes 221184 | tf_op jit(solution)/shard_map/all_gather | solution.py:126
  54.5 0.0 copy-done
  54.5 1.3 %convolution_convert_fusion = bf16[32,512]{1,0:T(8,128)(2,1)} fusion(bf16[32,3072]{1,0:T(8,128)(2,1)S(1)} %reshape.491, bf16[3072,512]{1,0:T(8,128)(2,1)S(1)} %copy-done), kind=kOutput, calls=%fused_computation.13 | convolution fusion | flops 100679680 | bytes 3375104 | tf_op jit(solution)/shard_map/dot_general | solution.py:125
  (10 shorter events, 0.1 us)
Async XLA Ops:
  0.6 53.9 %copy-start = (bf16[3072,512]{1,0:T(8,128)(2,1)S(1)}, bf16[3072,512]{1,0:T(8,128)(2,1)}, u32[]{:S(2)}) copy-start(bf16[3072,512]{1,0:T(8,128)(2,1)} %param.20) | copy-start | bytes 9437188
  17.1 13.1 %copy-start.3 = (f32[24]{0:T(128)S(1)}, f32[24]{0:T(128)}, u32[]{:S(2)}) copy-start(f32[24]{0:T(128)} %param.21) | copy-start | bytes 292
  17.1 13.1 %copy-start.4 = (s32[1,4]{1,0:T(1,128)S(1)}, s32[1,4]{1,0:T(1,128)}, u32[]{:S(2)}) copy-start(s32[1,4]{1,0:T(1,128)} %param.26) | copy-start | bytes 52
  17.1 14.2 %copy-start.1 = (bf16[1,4,3072]{2,1,0:T(4,128)(2,1)S(1)}, bf16[1,4,3072]{2,1,0:T(4,128)(2,1)}, u32[]{:S(2)}) copy-start(bf16[1,4,3072]{2,1,0:T(4,128)(2,1)} %param.23) | copy-start | bytes 73732
  17.1 14.2 %copy-start.2 = (bf16[1,4,3072]{2,1,0:T(4,128)(2,1)S(1)}, bf16[1,4,3072]{2,1,0:T(4,128)(2,1)}, u32[]{:S(2)}) copy-start(bf16[1,4,3072]{2,1,0:T(4,128)(2,1)} %param.24) | copy-start | bytes 73732
  24.1 11.4 %all-to-all-start = ((bf16[32,4,384]{2,1,0:T(4,128)(2,1)}), bf16[32,4,384]{2,1,0:T(4,128)(2,1)S(1)}, u32[]{:S(2)}, u32[]{:S(2)}) async-start(bf16[32,4,384]{2,1,0:T(4,128)(2,1)} %reshape.477), calls=%async_computation | async-start | bytes 196608 | tf_op jit(solution)/shard_map/all_to_all | solution.py:104
where the time goes:
time: 56.1 us; the launch traced here: 55.8 us
  blocking collectives  30.9 us (55%)
  matrix products  16.1 us (29%)
  starting transfers between devices  4.68 us (8%)
  between operations  2.12 us (4%)
  other arithmetic  1.07 us (2%)
  local copies, waits for them, and re-layouts  0.95 us (2%)
    all_gather x1, blocking collectives, per_device(): lax.all_gather(tokens, ('kv', 'tp'), axis=1, tiled=True).astype(jnp.float32)  16.3 us
    all_gather x1, blocking collectives, per_device(): lax.all_gather(mixed, ('kv', 'tp'), axis=0, tiled=True)  14.6 us
    dot_general x1, matrix products, per_device(): jnp.dot(full_normed, weights, preferred_element_type=jnp.float32)  6.34 us
    all_to_all x1, starting transfers between devices, per_device(): lax.all_to_all(projected, ('kv', 'tp'), split_axis=0, concat_axis=2, tile...  4.68 us
    dot_general x1, matrix products, advance(): jnp.einsum('bphd,bphe->bhde', old_keys * weights[..., None], old_values,...  4.16 us
    dot_general x1, matrix products, retain(): jnp.einsum('bihd,bhde->bihe', rotated_q, carried, precision=HIGH)  2.85 us
    dot_general x1, matrix products, per_device(): jnp.dot(lax.all_gather(mixed, ('kv', 'tp'), axis=0, tiled=True), w_output...  1.26 us
  transfers between devices with their start and end apart: 1, of which 0 were waited for; matrix products, arithmetic and copies ran while one was open for 10% of the time, Pallas kernels for 0%

commit v1 on v0

--- a/solution.py
+++ b/solution.py
@@ -101,7 +101,12 @@
     projected = jnp.dot(full_normed, weights, preferred_element_type=jnp.float32)
     rows_count = tokens.shape[0]
     projected = projected.astype(jnp.bfloat16).reshape(rows_count, 4, columns // 4)
-    regrouped = lax.all_to_all(projected, ("kv", "tp"), split_axis=0, concat_axis=2, tiled=True)
+    regrouped = jnp.concatenate(
+        lax.all_to_all(
+            jnp.stack(jnp.split(projected, lax.axis_size(("kv", "tp")), axis=0)), ("kv", "tp"), 0, 0
+        ),
+        axis=2,
+    )
     nseq = state.shape[0]
     heads = decay_rate.shape[0]
     head_dim = state.shape[2]

time: 56.1 us -> 60.5 us (1.078)
  local copies, waits for them, and re-layouts: 0.95 us -> 5.27 us
    unnamed x11 -> x18, local copies, waits for them, and re-layouts: 0.08 us -> 4.31 us
    another operation x0 -> x9, local copies, waits for them, and re-layouts: none -> 0.71 us  [per_device(): jnp.stack(jnp.split(projected, lax.axis_size(('kv', 'tp')), axis=0))]
    reshape x1, local copies, waits for them, and re-layouts: 0.65 us -> 0.04 us  [per_device(): jnp.concatenate(lax.all_to_all(jnp.stack(jnp.split(projected, lax.axis_si...]
  transfers between devices with their start and end apart: 1 -> 1, of which waited for: 0 -> 0; matrix products, arithmetic and copies ran while one was open for 10% -> 9% of each run, Pallas kernels for 0% -> 0%
where the time goes in v1:
time: 60.5 us; the launch traced here: 60.2 us
  blocking collectives  30.9 us (51%)
  matrix products  16.1 us (27%)
  local copies, waits for them, and re-layouts  5.27 us (9%)
  starting transfers between devices  4.68 us (8%)
  between operations  2.16 us (4%)
  other arithmetic  1.07 us (2%)
    all_gather x1, blocking collectives, per_device(): lax.all_gather(tokens, ('kv', 'tp'), axis=1, tiled=True).astype(jnp.float32)  16.3 us
    all_gather x1, blocking collectives, per_device(): lax.all_gather(mixed, ('kv', 'tp'), axis=0, tiled=True)  14.6 us
    dot_general x1, matrix products, per_device(): jnp.dot(full_normed, weights, preferred_element_type=jnp.float32)  6.34 us
    all_to_all x1, starting transfers between devices, per_device(): lax.all_to_all(jnp.stack(jnp.split(projected, lax.axis_size(('kv', 'tp'))...  4.68 us
    unnamed x18, local copies, waits for them, and re-layouts  4.31 us
    dot_general x1, matrix products, advance(): jnp.einsum('bphd,bphe->bhde', old_keys * weights[..., None], old_values,...  4.16 us
    dot_general x1, matrix products, retain(): jnp.einsum('bihd,bhde->bihe', rotated_q, carried, precision=HIGH)  2.85 us
    dot_general x1, matrix products, per_device(): jnp.dot(lax.all_gather(mixed, ('kv', 'tp'), axis=0, tiled=True), w_output...  1.26 us
  transfers between devices with their start and end apart: 1, of which 0 were waited for; matrix products, arithmetic and copies ran while one was open for 9% of the time, Pallas kernels for 0%

profile of v1, /device:TPU:0, one launch (start us, length us, event | category | flops | bytes accessed | tf_op | source)
XLA Modules:
  0.0 60.2 jit_solution(9756254841239469667)
XLA Ops:
  0.6 0.0 copy-start
  0.6 16.3 %all_gather.6 = bf16[32,4096]{1,0:T(8,128)(2,1)S(1)} all-gather(bf16[32,512]{1,0:T(8,128)(2,1)} %param.14), channel_id=1, replica_groups=mesh['dp'=4,'kv'=4,'tp'=2] {'kv','tp'}, dimensions={1}, use_global_device_ids=true | all-gather | bytes 294912 | tf_op jit(solution)/shard_map/all_gather | solution.py:98
  16.9 0.2 fusion.20
  17.1 0.0 copy-start.3
  17.1 0.0 copy-start.4
  17.1 0.0 copy-start.1
  17.1 0.0 copy-start.2
  17.1 6.3 %fusion.8 = bf16[32,1536]{1,0:T(8,128)(2,1)S(1)} fusion(bf16[4096,384]{1,0:T(8,128)(2,1)} %param.19, bf16[4096,384]{1,0:T(8,128)(2,1)} %param.18, bf16[4096,384]{1,0:T(8,128)(2,1)} %param.17, bf16[4096,384]{1,0:T(8,128)(2,1)} %param.16, bf16[32,4096]{1,0:T(8,128)(2,1)S(1)} %all_gather.6, f32[4096]{0:T(1024)} %param.15, f32[32]{0:T(128)S(1)} %add_rsqrt_fusion.1), kind=kOutput, calls=%fused_computation.8 | convolution fusion | flops 453558272 | bytes 12959872 | tf_op jit(solution)/shard_map/dot_general | solution.py:101
  23.7 0.6 %constant_dynamic-update-slice_fusion.7 = bf16[8,4,4,384]{3,2,1,0:T(4,128)(2,1)} fusion(bf16[1,4,4,384]{3,2,1,0:T(4,128)(2,1)S(1)} %stack.27), kind=kLoop, calls=%fused_computation.59 | loop fusion | bytes 24576
  24.3 0.6 %constant_dynamic-update-slice_fusion.6 = bf16[8,4,4,384]{3,2,1,0:T(4,128)(2,1)} fusion(bf16[8,4,4,384]{3,2,1,0:T(4,128)(2,1)} %constant_dynamic-update-slice_fusion.7, bf16[1,4,4,384]{3,2,1,0:T(4,128)(2,1)S(1)} %stack.28), kind=kLoop, calls=%fused_computation.58 | loop fusion | bytes 24576
  24.9 0.6 constant_dynamic-update-slice_fusion.5
  25.5 0.6 constant_dynamic-update-slice_fusion.4
  26.1 0.6 %constant_dynamic-update-slice_fusion.3 = bf16[8,4,4,384]{3,2,1,0:T(4,128)(2,1)} fusion(bf16[8,4,4,384]{3,2,1,0:T(4,128)(2,1)} %constant_dynamic-update-slice_fusion.4, bf16[1,4,4,384]{3,2,1,0:T(4,128)(2,1)S(1)} %stack.31), kind=kLoop, calls=%fused_computation.55 | loop fusion | bytes 24576
  26.7 0.6 %constant_dynamic-update-slice_fusion.2 = bf16[8,4,4,384]{3,2,1,0:T(4,128)(2,1)} fusion(bf16[8,4,4,384]{3,2,1,0:T(4,128)(2,1)} %constant_dynamic-update-slice_fusion.3, bf16[1,4,4,384]{3,2,1,0:T(4,128)(2,1)S(1)} %stack.32), kind=kLoop, calls=%fused_computation.54 | loop fusion | bytes 24576
  27.3 0.6 %constant_dynamic-update-slice_fusion.1 = bf16[8,4,4,384]{3,2,1,0:T(4,128)(2,1)} fusion(bf16[8,4,4,384]{3,2,1,0:T(4,128)(2,1)} %constant_dynamic-update-slice_fusion.2, bf16[1,4,4,384]{3,2,1,0:T(4,128)(2,1)S(1)} %stack.33), kind=kLoop, calls=%fused_computation.53 | loop fusion | bytes 24576
  27.9 0.6 constant_dynamic-update-slice_fusion
  28.5 4.7 %all-to-all-start = ((bf16[8,4,4,384]{3,2,1,0:T(4,128)(2,1)}), bf16[8,4,4,384]{3,2,1,0:T(4,128)(2,1)S(1)}, u32[]{:S(2)}, u32[]{:S(2)}) async-start(bf16[8,4,4,384]{3,2,1,0:T(4,128)(2,1)} %constant_dynamic-update-slice_fusion), calls=%async_computation | async-start | bytes 196608 | tf_op jit(solution)/shard_map/all_to_all | solution.py:105
  34.5 0.0 copy-done.3
  34.5 0.0 copy-done.4
  34.6 0.3 fusion.39
  34.8 0.3 fusion.38
  35.1 0.3 fusion.51
  35.3 0.1 copy.40
  35.4 0.1 multiply_cosine_fusion
  35.6 0.1 multiply_exponential_fusion
  35.6 0.0 copy-done.1
  35.6 0.0 copy-done.2
  35.7 4.2 %bitcast_add_fusion = f32[1,24,128,128]{3,2,1,0:T(8,128)} fusion(f32[1,24,128,128]{3,2,1,0:T(8,128)} %param.22, f32[24]{0:T(128)S(1)} %get-tuple-element.31, bf16[1,4,3072]{2,1,0:T(4,128)(2,1)S(1)} %copy-done.1, bf16[1,4,3072]{2,1,0:T(4,128)(2,1)S(1)} %copy-done.2, f32[4,24]{0,1:T(8,128)S(1)} %get-tuple-element.29), kind=kOutput, calls=%fused_computation.11 | convolution fusion | flops 19685376 | bytes 3195360 | tf_op jit(solution)/shard_map/bphd,bphe->bhde/dot_general | solution.py:51
  39.8 0.1 subtract_maximum_fusion
  39.9 0.0 all-to-all-done
  39.9 0.2 slice_reduce_fusion
  40.2 0.1 fusion.48
  40.3 0.1 subtract_bitcast_fusion
  40.3 2.9 %fusion.17 = f32[1,4,24,128]{3,1,2,0:T(4,128)S(1)} fusion(f32[1,24,128,128]{3,2,1,0:T(8,128)} %bitcast_add_fusion, f32[4,24]{0,1:T(8,128)S(1)} %get-tuple-element.28, f32[1,4,24,64]{3,1,2,0:T(4,128)S(1)} %get-tuple-element.22, f32[1,4,24,64]{3,1,2,0:T(4,128)S(1)} %get-tuple-element.23), kind=kOutput, calls=%fused_computation.17 | convolution fusion | flops 18898944 | bytes 1671552 | tf_op jit(solution)/shard_map/bihd,bhde->bihe/dot_general | solution.py:69
  43.2 0.4 convolution_multiply_fusion
  43.6 0.3 fusion.52
  43.9 0.2 multiply_reduce_fusion
  44.1 0.1 fusion.37
  44.2 14.6 %all-gather = bf16[8,4,3072]{2,1,0:T(4,128)(2,1)S(1)} all-gather(bf16[1,4,3072]{2,1,0:T(4,128)(2,1)S(1)} %fusion.37), channel_id=1, replica_groups=mesh['dp'=4,'kv'=4,'tp'=2] {'kv','tp'}, dimensions={0}, use_global_device_ids=true | all-gather | bytes 221184 | tf_op jit(solution)/shard_map/all_gather | solution.py:131
  58.9 0.0 copy-done
  58.9 1.3 %convolution_convert_fusion = bf16[32,512]{1,0:T(8,128)(2,1)} fusion(bf16[32,3072]{1,0:T(8,128)(2,1)S(1)} %reshape.512, bf16[3072,512]{1,0:T(8,128)(2,1)S(1)} %copy-done), kind=kOutput, calls=%fused_computation.13 | convolution fusion | flops 100679680 | bytes 3375104 | tf_op jit(solution)/shard_map/dot_general | solution.py:130
  (19 shorter events, 0.3 us)
Async XLA Ops:
  0.6 58.3 %copy-start = (bf16[3072,512]{1,0:T(8,128)(2,1)S(1)}, bf16[3072,512]{1,0:T(8,128)(2,1)}, u32[]{:S(2)}) copy-start(bf16[3072,512]{1,0:T(8,128)(2,1)} %param.20) | copy-start | bytes 9437188
  17.1 17.4 %copy-start.3 = (f32[24]{0:T(128)S(1)}, f32[24]{0:T(128)}, u32[]{:S(2)}) copy-start(f32[24]{0:T(128)} %param.21) | copy-start | bytes 292
  17.1 17.5 %copy-start.4 = (s32[1,4]{1,0:T(1,128)S(1)}, s32[1,4]{1,0:T(1,128)}, u32[]{:S(2)}) copy-start(s32[1,4]{1,0:T(1,128)} %param.26) | copy-start | bytes 52
  17.1 18.5 %copy-start.1 = (bf16[1,4,3072]{2,1,0:T(4,128)(2,1)S(1)}, bf16[1,4,3072]{2,1,0:T(4,128)(2,1)}, u32[]{:S(2)}) copy-start(bf16[1,4,3072]{2,1,0:T(4,128)(2,1)} %param.23) | copy-start | bytes 73732
  17.1 18.5 %copy-start.2 = (bf16[1,4,3072]{2,1,0:T(4,128)(2,1)S(1)}, bf16[1,4,3072]{2,1,0:T(4,128)(2,1)}, u32[]{:S(2)}) copy-start(bf16[1,4,3072]{2,1,0:T(4,128)(2,1)} %param.24) | copy-start | bytes 73732
  28.5 11.4 %all-to-all-start = ((bf16[8,4,4,384]{3,2,1,0:T(4,128)(2,1)}), bf16[8,4,4,384]{3,2,1,0:T(4,128)(2,1)S(1)}, u32[]{:S(2)}, u32[]{:S(2)}) async-start(bf16[8,4,4,384]{3,2,1,0:T(4,128)(2,1)} %constant_dynamic-update-slice_fusion), calls=%async_computation | async-start | bytes 196608 | tf_op jit(solution)/shard_map/all_to_all | solution.py:105
